TPU v7x, 128 devices: a whole 4x4x4 slice. The times are simulated.
128 devices in a mesh: ep: 128 (over z, y, x, core).
Axes of the slice: x: 4, y: 4, z: 4, core: 2. Of those that a mesh axis runs over, the one named last changes fastest.
Arguments:
- tokens: bfloat16 [512, 2048], P('ep'), may hold values from -6 to 6
- lengths: int32 [512], P('ep'), may hold values from 1 to 1023
- cache_keys: bfloat16 [512, 1024, 2, 128], P('ep')
- cache_values: bfloat16 [512, 1024, 2, 128], P('ep'), may hold values from -6 to 6
- query_w: bfloat16 [2048, 1024], replicated, may hold values from -0.125 to 0.125
- key_w: bfloat16 [2048, 256], replicated, may hold values from -0.125 to 0.125
- value_w: bfloat16 [2048, 256], replicated, may hold values from -0.125 to 0.125
- out_w: bfloat16 [1024, 2048], replicated, may hold values from -0.1875 to 0.1875
- mix_lambda: float32 [8], replicated, may hold values from 0.3 to 0.8
- head_gain: float32 [128], replicated, may hold values from 0.1 to 1.9
- attn_gain: float32 [2048], replicated, may hold values from 0.1 to 1.9
- ffn_gain: float32 [2048], replicated, may hold values from 0.1 to 1.9
- routes: int32 [512, 2], P('ep'), may hold values from 0 to 7, all different within a row; in each aligned block of 4 rows (0 to 3, 4 to 7, ...) at most 2 rows name the same one
- route_weights: float32 [512, 2], P('ep'), may hold values from 0.2 to 1
- exp_gate: bfloat16 [2048, 49152], P(None, 'ep'), may hold values from -0.125 to 0.125
- exp_up: bfloat16 [2048, 49152], P(None, 'ep'), may hold values from -0.125 to 0.125
- exp_down: bfloat16 [49152, 2048], P('ep'), may hold values from -0.078125 to 0.078125
- dense_gate: bfloat16 [128, 256, 352], P('ep'), may hold values from -0.125 to 0.125
- dense_up: bfloat16 [128, 256, 352], P('ep'), may hold values from -0.125 to 0.125
- dense_down: bfloat16 [128, 352, 256], P('ep'), may hold values from -0.078125 to 0.078125
- branch_gate: bfloat16 [2048], replicated, may hold values from -0.125 to 0.125
Outputs:
- output: bfloat16 [512, 2048], P('ep')
- new_keys: bfloat16 [512, 256], P('ep')
- new_values: bfloat16 [512, 256], P('ep')
Inputs may be any that keep to these rules, and one draw needn't show every extreme that they name: `routes`: each row names 2 different experts; among the 4 rows of one device no expert is named by more than 2 rows, a bound that some block reaches.
All inputs are finite; a program needn't handle non-finite values.
Results may differ from a plain program's by a relative error of at most 0.015.
Values may be sent and summed in bfloat16 or wider, within the bound.
A program may use at most 128 MiB of HBM per device.

v0:
```python
import jax
import jax.numpy as jnp
from jax import lax
from jax.sharding import PartitionSpec as P

HEADS = 8
KV_HEADS = 2
HEAD_DIM = 128
SEQ_DEV = 4
TOP_K = 2
SPLIT = 16


def sent_together(arrays, axis, split_dim, concat_dim, along):
    widths = [a.shape[along] for a in arrays]
    both = jnp.concatenate(arrays, axis=along)
    filled = lax.all_to_all(both, axis, split_axis=split_dim, concat_axis=concat_dim, tiled=True)
    return tuple(jnp.split(filled, [sum(widths[:k]) for k in range(1, len(widths))], axis=along))


def split_up(x, dim, peers):
    before, after = (x.shape[:dim], x.shape[dim + 1 :])
    return jnp.moveaxis(x.reshape(*before, peers, -1, *after), dim, 0)


def cut_rows(length, count):
    unit = 8 if length >= 8 * count else 1
    return [length // unit * k // count * unit for k in range(1, count)]


def in_order(tiles, dim):
    lengths = list(tiles.shape[1:])
    lengths[dim] *= tiles.shape[0]
    return jnp.moveaxis(tiles, 0, dim).reshape(lengths)


def exchange_in_pieces(x, axis, pieces, split_dim, concat_dim):
    tiles = split_up(x, split_dim, lax.axis_size(axis))
    cut = max(range(1, max(2, tiles.ndim - 1)), key=lambda d: tiles.shape[d])
    outs = []
    for piece in jnp.split(tiles, cut_rows(tiles.shape[cut], pieces), axis=cut):
        if piece.size:
            outs.append(lax.all_to_all(piece, axis, split_axis=0, concat_axis=0, tiled=True))
    return in_order(jnp.concatenate(outs, axis=cut), concat_dim)


def rms_norm(values, gain, epsilon):
    scale = lax.rsqrt(jnp.mean(values * values, axis=-1, keepdims=True) + epsilon)
    return values * scale * gain


def softmax_pair(scores, own_score, valid):
    masked = jnp.where(valid, scores, -jnp.inf)
    largest = jnp.maximum(jnp.max(masked, axis=-1), own_score)
    raised = jnp.where(valid, jnp.exp(scores - largest[..., None]), 0.0)
    own_raised = jnp.exp(own_score - largest)
    total = jnp.sum(raised, axis=-1) + own_raised
    return (raised / total[..., None], own_raised / total)


def swiglu_rows(chosen, w_gate, w_up, w_down):
    gate_part = jnp.dot(chosen, w_gate, preferred_element_type=jnp.float32)
    up_part = jnp.dot(chosen, w_up, preferred_element_type=jnp.float32)
    act = (jax.nn.silu(gate_part) * up_part).astype(jnp.bfloat16)
    return jnp.dot(act, w_down, preferred_element_type=jnp.float32)


def per_device(
    tokens,
    lengths,
    cache_keys,
    cache_values,
    query_w,
    key_w,
    value_w,
    out_w,
    mix_lambda,
    head_gain,
    attn_gain,
    ffn_gain,
    routes,
    route_weights,
    exp_gate,
    exp_up,
    exp_down,
    dense_gate,
    dense_up,
    dense_down,
    branch_gate,
):
    rows = tokens.shape[0]
    groups = HEADS // KV_HEADS
    half = HEAD_DIM // 2
    scale = (HEAD_DIM // 2) ** (-0.5)
    cache_len = cache_keys.shape[1]
    xfull = tokens.astype(jnp.float32)
    normed = rms_norm(xfull, attn_gain, 1e-06).astype(jnp.bfloat16)
    query = jnp.dot(normed, query_w, preferred_element_type=jnp.float32).astype(jnp.bfloat16)
    key_new = jnp.dot(normed, key_w, preferred_element_type=jnp.float32).astype(jnp.bfloat16)
    value_new = jnp.dot(normed, value_w, preferred_element_type=jnp.float32).astype(jnp.bfloat16)
    qheads = query.reshape(rows, KV_HEADS, groups, HEAD_DIM)
    knew = key_new.reshape(rows, KV_HEADS, HEAD_DIM)
    vnew = value_new.reshape(rows, KV_HEADS, HEAD_DIM)
    valid = (jnp.arange(cache_len, dtype=jnp.int32)[None, :] < lengths[:, None])[:, None, None, :]
    first = (
        jnp.einsum(
            "sgqd,spgd->sgqp",
            qheads[..., :half],
            cache_keys[..., :half],
            preferred_element_type=jnp.float32,
        )
        * scale
    )
    first_own = (
        jnp.einsum(
            "sgqd,sgd->sgq",
            qheads[..., :half],
            knew[..., :half],
            preferred_element_type=jnp.float32,
        )
        * scale
    )
    second = (
        jnp.einsum(
            "sgqd,spgd->sgqp",
            qheads[..., half:],
            cache_keys[..., half:],
            preferred_element_type=jnp.float32,
        )
        * scale
    )
    second_own = (
        jnp.einsum(
            "sgqd,sgd->sgq",
            qheads[..., half:],
            knew[..., half:],
            preferred_element_type=jnp.float32,
        )
        * scale
    )
    prob_one, own_one = softmax_pair(first, first_own, valid)
    prob_two, own_two = softmax_pair(second, second_own, valid)
    lam = mix_lambda.reshape(KV_HEADS, groups)
    weights = (prob_one - lam[None, :, :, None] * prob_two).astype(jnp.bfloat16)
    own_weights = (own_one - lam[None] * own_two).astype(jnp.bfloat16)
    mixed = jnp.einsum("sgqp,spgd->sgqd", weights, cache_values, preferred_element_type=jnp.float32)
    mixed = (
        mixed + own_weights.astype(jnp.float32)[..., None] * vnew.astype(jnp.float32)[:, :, None, :]
    )
    heads = rms_norm(mixed, head_gain, 1e-05).astype(jnp.bfloat16).reshape(rows, HEADS * HEAD_DIM)
    hidden_state = xfull + jnp.dot(heads, out_w, preferred_element_type=jnp.float32)
    ffn_in = rms_norm(hidden_state, ffn_gain, 1e-06).astype(jnp.bfloat16)
    devices = lax.axis_size("ep")
    experts = devices // SPLIT
    row_blocks = devices // SPLIT
    capacity = min(SEQ_DEV, max(2, SEQ_DEV * TOP_K * 2 // experts))
    slots = jnp.arange(capacity, dtype=jnp.int32)
    all_rows = lax.all_gather(ffn_in, "ep", axis=0, tiled=True)
    gate = jax.nn.sigmoid(jnp.dot(ffn_in, branch_gate, preferred_element_type=jnp.float32))
    position = lax.axis_index("ep")
    row_span = dense_gate.shape[1]
    col_span = dense_gate.shape[2]
    row_block = position // SPLIT
    columns = lax.dynamic_slice_in_dim(all_rows, row_block * row_span, row_span, 1)
    gate_tile = jnp.dot(columns, dense_gate[0], preferred_element_type=jnp.float32).reshape(
        devices, rows, col_span
    )
    up_tile = jnp.dot(columns, dense_up[0], preferred_element_type=jnp.float32).reshape(
        devices, rows, col_span
    )
    gate_in, up_in = tuple(
        (
            part.astype(jnp.float32)
            for part in sent_together(
                (gate_tile.astype(jnp.bfloat16), up_tile.astype(jnp.bfloat16)), "ep", 0, 0, 1
            )
        )
    )
    gate_sum = jnp.sum(gate_in.reshape(row_blocks, SPLIT, rows, col_span), axis=0)
    up_sum = jnp.sum(up_in.reshape(row_blocks, SPLIT, rows, col_span), axis=0)
    own_act = (jax.nn.silu(gate_sum) * up_sum).astype(jnp.bfloat16)
    outgoing_act = jnp.tile(own_act, (row_blocks, 1, 1))
    act_in = lax.all_to_all(outgoing_act, "ep", split_axis=0, concat_axis=0, tiled=True)
    down_tile = jnp.dot(
        act_in.reshape(devices * rows, col_span), dense_down[0], preferred_element_type=jnp.float32
    )
    down_in = lax.all_to_all(
        down_tile.reshape(devices, rows, row_span).astype(jnp.bfloat16),
        "ep",
        split_axis=0,
        concat_axis=0,
        tiled=True,
    ).astype(jnp.float32)
    down_sum = jnp.sum(down_in.reshape(row_blocks, SPLIT, rows, row_span), axis=1)
    dense = jnp.transpose(down_sum, (1, 0, 2)).reshape(rows, row_blocks * row_span)
    expert_ids = jnp.arange(experts, dtype=jnp.int32)
    match = routes[None, :, :] == expert_ids[:, None, None]
    weight = jnp.sum(jnp.where(match, route_weights[None], 0.0), axis=-1)
    hit = jnp.any(match, axis=-1).astype(jnp.int32)
    rank = jnp.cumsum(hit, axis=1) - 1
    select = (hit[:, None, :] == 1) & (rank[:, None, :] == slots[None, :, None])
    chosen = jnp.einsum(
        "ecs,sd->ecd", select.astype(jnp.bfloat16), ffn_in, preferred_element_type=jnp.float32
    ).astype(jnp.bfloat16)
    outgoing = jnp.repeat(chosen, SPLIT, axis=0)
    incoming = lax.all_to_all(outgoing, "ep", split_axis=0, concat_axis=0, tiled=True)
    sources = incoming.shape[0]
    taken = incoming.shape[1]
    result = swiglu_rows(incoming.reshape(sources * taken, -1), exp_gate, exp_up, exp_down)
    returned = exchange_in_pieces(
        result.reshape(sources, taken, -1).astype(jnp.bfloat16), "ep", 2, 0, 0
    ).astype(jnp.float32)
    summed = jnp.sum(returned.reshape(experts, SPLIT, capacity, -1), axis=1)
    weighted = select.astype(jnp.float32) * weight[:, None, :]
    routed = jnp.einsum("ecs,ecd->sd", weighted, summed, precision=lax.Precision.HIGHEST)
    output = (hidden_state + routed + gate[:, None] * dense).astype(jnp.bfloat16)
    return (output, key_new, value_new)


def solution(mesh):
    placed = (
        P("ep", None),
        P("ep"),
        P("ep", None, None, None),
        P("ep", None, None, None),
        P(),
        P(),
        P(),
        P(),
        P(),
        P(),
        P(),
        P(),
        P("ep", None),
        P("ep", None),
        P(None, "ep"),
        P(None, "ep"),
        P("ep", None),
        P("ep", None, None),
        P("ep", None, None),
        P("ep", None, None),
        P(),
    )
    return jax.shard_map(
        per_device,
        mesh=mesh,
        in_specs=placed,
        out_specs=(P("ep", None), P("ep", None), P("ep", None)),
        check_vma=False,
    )
```

profile of v0, /device:TPU:1, one launch (start us, length us, event | category | flops | bytes accessed | tf_op | source)
XLA Modules:
  0.0 199.1 jit_solution(3395068889452520648)
XLA Ops:
  7.2 1.0 fusion.47
  8.2 2.9 %convolution_convert_fusion.5 = bf16[4,1024]{1,0:T(4,128)(2,1)S(1)} fusion(bf16[2048,1024]{1,0:T(8,128)(2,1)} %param.25, bf16[4,2048]{1,0:T(4,128)(2,1)} %param.21, f32[2048]{0:T(1024)} %param.31, f32[4]{0:T(128)S(1)} %add_rsqrt_fusion.2), kind=kOutput, calls=%fused_computation.22 | convolution fusion | flops 16814080 | bytes 4227088 | tf_op jit(solution)/shard_map/dot_general | solution.py:98
  11.2 0.1 iota_compare_fusion
  11.3 6.8 %fusion.79 = (bf16[4,1024,2,64]{3,2,1,0:T(2,128)(2,1)}, bf16[4,1024,2,64]{3,2,1,0:T(2,128)(2,1)}) fusion(bf16[4,1024,2,128]{3,2,1,0:T(2,128)(2,1)} %param.23), kind=kLoop, calls=%fused_computation.114 | loop fusion | bytes 4194304 | tf_op jit(solution)/shard_map/slice | solution.py:127
  18.1 0.3 convolution_convert_fusion.7
  18.4 0.1 slice_bitcast_fusion
  18.5 0.1 fusion.54
  18.6 0.2 fusion.51
  18.8 0.1 mul.148
  18.9 0.3 convolution_convert_fusion.6
  19.2 2.5 %select_reduce_fusion.1 = (f32[4,2,4]{2,1,0:T(2,128)S(1)}, f32[4,2,4,1024]{3,2,1,0:T(4,128)S(1)}) fusion(pred[4,1024]{1,0:T(4,128)(4,1)S(1)} %iota_compare_fusion, bf16[4,1024,2,64]{3,2,1,0:T(2,128)(2,1)} %get-tuple-element.6, bf16[4,2,4,128]{3,2,1,0:T(4,128)(2,1)S(1)} %reshape.159), kind=kOutput, calls=%fused_computation.52 | convolution fusion | flops 4292576 | bytes 1192064 | tf_op jit(solution)/shard_map/sgqd,spgd->sgqp/dot_general | solution.py:106
  21.7 0.8 fusion.37
  22.5 0.2 fusion.38
  22.8 0.6 multiply_reduce_fusion.1
  23.4 0.1 multiply_convert_fusion.2
  23.5 3.0 %multiply_reduce_fusion = (f32[4]{0:T(128)S(1)}, f32[4,2048]{1,0:T(4,128)S(1)}) fusion(bf16[4,1024]{1,0:T(4,128)(2,1)S(1)} %reshape.161, bf16[1024,2048]{1,0:T(8,128)(2,1)} %param.28, bf16[4,2048]{1,0:T(4,128)(2,1)S(1)} %copy-done.6), kind=kOutput, calls=%fused_computation.70 | convolution fusion | flops 16809980 | bytes 4251664 | tf_op jit(solution)/shard_map/dot_general | solution.py:151
  26.5 0.7 fusion.95
  27.2 0.1 fusion.58
  27.4 0.1 multiply_convert_fusion.1
  27.4 0.2 convolution_convert_fusion.1
  27.6 0.1 copy.78
  27.7 1.6 broadcast_in_dim.69
  29.3 12.0 %all-to-all-start = ((bf16[128,2,2048]{2,1,0:T(2,128)(2,1)}), bf16[128,2,2048]{2,1,0:T(2,128)(2,1)}, u32[]{:S(2)}, u32[]{:S(2)}) async-start(bf16[128,2,2048]{2,1,0:T(2,128)(2,1)} %bitcast.7), calls=%async_computation | async-start | bytes 2097152 | tf_op jit(solution)/shard_map/all_to_all | solution.py:206
  41.3 19.0 %all-to-all-done = bf16[128,2,2048]{2,1,0:T(2,128)(2,1)} async-done(((bf16[128,2,2048]{2,1,0:T(2,128)(2,1)}), bf16[128,2,2048]{2,1,0:T(2,128)(2,1)}, u32[]{:S(2)}, u32[]{:S(2)}) %all-to-all-start) | async-done | bytes 1048608 | tf_op jit(solution)/shard_map/all_to_all | solution.py:206
  60.4 1.5 reshape.163
  61.9 2.9 %fusion.82 = f32[256,384]{1,0:T(8,128)} fusion(bf16[256,2048]{1,0:T(8,128)(2,1)S(1)} %reshape.163, bf16[2048,384]{1,0:T(8,128)(2,1)} %param.35), kind=kOutput, calls=%fused_computation.117 | convolution fusion | flops 402653184 | bytes 3014656 | tf_op jit(solution)/shard_map/dot_general | solution.py:62
  64.7 4.4 %convolution_convert_fusion = bf16[256,2048]{1,0:T(8,128)(2,1)} fusion(bf16[384,2048]{1,0:T(8,128)(2,1)} %param.37, bf16[256,2048]{1,0:T(8,128)(2,1)S(1)} %reshape.163, bf16[2048,384]{1,0:T(8,128)(2,1)} %param.36, f32[256,384]{1,0:T(8,128)} %fusion.82), kind=kOutput, calls=%fused_computation | convolution fusion | flops 806420480 | bytes 5636096 | tf_op jit(solution)/shard_map/dot_general | solution.py:65
  69.1 1.7 convert_element_type.121
  70.8 2.5 %fusion.80 = (bf16[128,1,1,2048]{3,2,1,0:T(2,128)(2,1)}, bf16[128,1,1,2048]{3,2,1,0:T(2,128)(2,1)}) fusion(bf16[128,1,2,2048]{3,2,1,0:T(2,128)(2,1)S(1)} %bitcast.73), kind=kLoop, calls=%fused_computation.115 | loop fusion | bytes 2097152 | tf_op jit(solution)/shard_map/split | solution.py:41
  73.4 0.5 broadcast.142
  73.9 4.7 %reduce = bf16[128,2048]{1,0:T(8,128)(2,1)S(1)} reduce(bf16[128,1,1,2048]{3,2,1,0:T(2,128)(2,1)} %get-tuple-element.8, bf16[]{:T(256)} %broadcast.142), dimensions={1,2}, to_apply=%get-tuple-element.8.reduce_sub_computation | reduce | bytes 1048578 | tf_op jit(solution)/shard_map/split | solution.py:41
  78.6 1.2 reshape.192
  79.8 5.4 %all-to-all-start.2 = ((bf16[128,2,1024]{2,1,0:T(2,128)(2,1)}), bf16[128,2,1024]{2,1,0:T(2,128)(2,1)}, u32[]{:S(2)}, u32[]{:S(2)}) async-start(bf16[128,2,1024]{2,1,0:T(2,128)(2,1)} %reshape.192), calls=%async_computation.2 | async-start | bytes 1048576 | tf_op jit(solution)/shard_map/all_to_all | solution.py:43
  85.2 19.9 %all-gather.3.cloned.1.call-done = bf16[128,4,2048]{2,1,0:T(4,128)(2,1)} async-done(((bf16[1,4,2048]{2,1,0:T(4,128)(2,1)}), bf16[128,4,2048]{2,1,0:T(4,128)(2,1)}) %all-gather.3.cloned.1.call-update) | async-done | bytes 2097168 | tf_op jit(solution)/shard_map/all_gather | solution.py:158
  105.1 4.0 %reshape.180 = bf16[512,2048]{1,0:T(8,128)(2,1)} reshape(bf16[128,4,2048]{2,1,0:T(4,128)(2,1)} %all-gather.3.cloned.1.call-done) | data formatting | bytes 4194304
  109.0 1.0 constant_dynamic-slice_fusion
  110.0 0.1 dot_general.71
  110.1 0.3 convolution_convert_fusion.2
  110.4 0.3 convolution_convert_fusion.3
  110.7 0.9 pad_maximum_fusion.1
  111.6 2.4 %copy.84 = bf16[128,8,352]{2,1,0:T(8,128)(2,1)} copy(bf16[128,8,352]{0,2,1:T(8,128)(2,1)} %pad_maximum_fusion.1) | data formatting | bytes 1441792 | tf_op jit(solution)/shard_map/concatenate | solution.py:16
  114.1 6.1 %all-to-all-start.3 = ((bf16[128,8,352]{2,1,0:T(8,128)(2,1)}), bf16[128,8,352]{2,1,0:T(8,128)(2,1)}, u32[]{:S(2)}, u32[]{:S(2)}) async-start(bf16[128,8,352]{2,1,0:T(8,128)(2,1)} %copy.84), calls=%async_computation.3 | async-start | bytes 1572864 | tf_op jit(solution)/shard_map/all_to_all | solution.py:17
  120.2 4.4 %reduce.1 = bf16[128,2048]{1,0:T(8,128)(2,1)} reduce(bf16[128,1,1,2048]{3,2,1,0:T(2,128)(2,1)S(1)} %copy-done.1, bf16[]{:T(256)} %broadcast.142), dimensions={1,2}, to_apply=%get-tuple-element.7.reduce_sub_computation | reduce | bytes 1048578 | tf_op jit(solution)/shard_map/split | solution.py:41
  124.6 2.2 %reshape.194 = bf16[128,2,1024]{2,1,0:T(2,128)(2,1)} reshape(bf16[128,2048]{1,0:T(8,128)(2,1)} %reduce.1) | data formatting | bytes 1048576
  126.8 9.4 %all-to-all-done.3 = bf16[128,8,352]{2,1,0:T(8,128)(2,1)} async-done(((bf16[128,8,352]{2,1,0:T(8,128)(2,1)}), bf16[128,8,352]{2,1,0:T(8,128)(2,1)}, u32[]{:S(2)}, u32[]{:S(2)}) %all-to-all-start.3) | async-done | bytes 720928 | tf_op jit(solution)/shard_map/all_to_all | solution.py:17
  136.3 4.5 %all-to-all-start.1 = ((bf16[128,2,1024]{2,1,0:T(2,128)(2,1)}), bf16[128,2,1024]{2,1,0:T(2,128)(2,1)S(1)}, u32[]{:S(2)}, u32[]{:S(2)}) async-start(bf16[128,2,1024]{2,1,0:T(2,128)(2,1)} %reshape.194), calls=%async_computation.1 | async-start | bytes 1048576 | tf_op jit(solution)/shard_map/all_to_all | solution.py:43
  140.8 1.7 fusion.81
  142.6 0.1 convert_reduce_fusion.1
  142.8 1.1 copy.87
  143.9 10.5 %all-to-all-done.1 = bf16[128,2,1024]{2,1,0:T(2,128)(2,1)S(1)} async-done(((bf16[128,2,1024]{2,1,0:T(2,128)(2,1)}), bf16[128,2,1024]{2,1,0:T(2,128)(2,1)S(1)}, u32[]{:S(2)}, u32[]{:S(2)}) %all-to-all-start.1) | async-done | bytes 524320 | tf_op jit(solution)/shard_map/all_to_all | solution.py:43
  154.4 5.4 %all-to-all-start.4 = ((bf16[128,4,352]{2,1,0:T(4,128)(2,1)}), bf16[128,4,352]{2,1,0:T(4,128)(2,1)}, u32[]{:S(2)}, u32[]{:S(2)}) async-start(bf16[128,4,352]{2,1,0:T(4,128)(2,1)} %copy.87), calls=%async_computation.4 | async-start | bytes 786432 | tf_op jit(solution)/shard_map/all_to_all | solution.py:183
  159.8 0.1 select_reduce_fusion.2
  159.9 0.1 fusion.22
  160.0 3.6 %reshape.193 = bf16[128,1,1,2048]{3,2,1,0:T(2,128)(2,1)S(1)} reshape(bf16[128,2,1024]{2,1,0:T(2,128)(2,1)} %all-to-all-done.2) | data formatting | bytes 1048576
  163.6 4.4 %reshape.195 = bf16[128,1,1,2048]{3,2,1,0:T(2,128)(2,1)} reshape(bf16[128,2,1024]{2,1,0:T(2,128)(2,1)} %copy-done.2) | data formatting | bytes 1048576
  168.0 3.8 %all-to-all-done.4 = bf16[128,4,352]{2,1,0:T(4,128)(2,1)} async-done(((bf16[128,4,352]{2,1,0:T(4,128)(2,1)}), bf16[128,4,352]{2,1,0:T(4,128)(2,1)}, u32[]{:S(2)}, u32[]{:S(2)}) %all-to-all-start.4) | async-done | bytes 360480 | tf_op jit(solution)/shard_map/all_to_all | solution.py:183
  171.8 1.3 convolution_convert_fusion.4
  173.2 0.9 copy.89
  174.1 6.1 %all-to-all-start.5 = ((bf16[128,4,256]{2,1,0:T(4,128)(2,1)}), bf16[128,4,256]{2,1,0:T(4,128)(2,1)S(1)}, u32[]{:S(2)}, u32[]{:S(2)}) async-start(bf16[128,4,256]{2,1,0:T(4,128)(2,1)} %copy.89), calls=%async_computation.5 | async-start | bytes 524288 | tf_op jit(solution)/shard_map/all_to_all | solution.py:187
  180.1 3.5 %pad_maximum_fusion = bf16[128,1,2,2048]{3,2,1,0:T(2,128)(2,1)S(1)} fusion(bf16[128,1,1,2048]{3,2,1,0:T(2,128)(2,1)S(1)} %reshape.193, bf16[128,1,1,2048]{3,2,1,0:T(2,128)(2,1)} %reshape.195), kind=kLoop, calls=%fused_computation.30 | loop fusion | flops 2097152 | bytes 2097152 | tf_op jit(solution)/shard_map/concatenate | solution.py:44
  183.6 0.8 convert_reduce_fusion
  184.5 6.8 %all-to-all-done.5 = bf16[128,4,256]{2,1,0:T(4,128)(2,1)S(1)} async-done(((bf16[128,4,256]{2,1,0:T(4,128)(2,1)}), bf16[128,4,256]{2,1,0:T(4,128)(2,1)S(1)}, u32[]{:S(2)}, u32[]{:S(2)}) %all-to-all-start.5) | async-done | bytes 262176 | tf_op jit(solution)/shard_map/all_to_all | solution.py:187
  191.2 0.1 convert_reduce_fusion.3
  191.3 0.9 fusion.2
  (59 shorter events, 0.6 us)
Async XLA Ops:
  7.2 15.6 %copy-start = (bf16[4,1024,2,128]{3,2,1,0:T(2,128)(2,1)S(1)}, bf16[4,1024,2,128]{3,2,1,0:T(2,128)(2,1)}, u32[]{:S(2)}) copy-start(bf16[4,1024,2,128]{3,2,1,0:T(2,128)(2,1)} %param.24) | copy-start | bytes 6291460
  7.2 97.9 %all-gather.3.cloned.1.call-start = ((), (), s32[]{:S(2)}) async-start(), calls=%async_computation.6 | async-start | bytes 2113536 | tf_op jit(solution)/shard_map/all_gather | solution.py:158
  8.2 2.9 %copy-start.17 = (s32[4]{0:T(128)S(1)}, s32[4]{0:T(128)}, u32[]{:S(2)}) copy-start(s32[4]{0:T(128)} %param.22) | copy-start | bytes 52
  11.3 6.8 %copy-start.4 = (bf16[2048,256]{1,0:T(8,128)(2,1)S(1)}, bf16[2048,256]{1,0:T(8,128)(2,1)}, u32[]{:S(2)}) copy-start(bf16[2048,256]{1,0:T(8,128)(2,1)} %param.26) | copy-start | bytes 3145732
  11.3 6.8 %copy-start.6 = (bf16[4,2048]{1,0:T(4,128)(2,1)S(1)}, bf16[4,2048]{1,0:T(4,128)(2,1)}, u32[]{:S(2)}) copy-start(bf16[4,2048]{1,0:T(4,128)(2,1)} %param.21) | copy-start | bytes 49156
  11.3 6.8 %copy-start.9 = (f32[2048]{0:T(1024)S(1)}, f32[2048]{0:T(1024)}, u32[]{:S(2)}) copy-start(f32[2048]{0:T(1024)} %param.31) | copy-start | bytes 24580
  11.3 7.5 %copy-start.18 = (f32[8]{0:T(128)S(1)}, f32[8]{0:T(128)}, u32[]{:S(2)}) copy-start(f32[8]{0:T(128)} %param.29) | copy-start | bytes 100
  11.3 7.6 %copy-start.5 = (bf16[2048,256]{1,0:T(8,128)(2,1)S(1)}, bf16[2048,256]{1,0:T(8,128)(2,1)}, u32[]{:S(2)}) copy-start(bf16[2048,256]{1,0:T(8,128)(2,1)} %param.27) | copy-start | bytes 3145732
  18.4 4.1 %copy-start.12 = (bf16[4,256]{1,0:T(4,128)(2,1)}, bf16[4,256]{1,0:T(4,128)(2,1)S(1)}, u32[]{:S(2)}) copy-start(bf16[4,256]{1,0:T(4,128)(2,1)S(1)} %convolution_convert_fusion.7) | copy-start | bytes 6148
  19.1 3.3 %copy-start.11 = (bf16[4,256]{1,0:T(4,128)(2,1)}, bf16[4,256]{1,0:T(4,128)(2,1)S(1)}, u32[]{:S(2)}) copy-start(bf16[4,256]{1,0:T(4,128)(2,1)S(1)} %convolution_convert_fusion.6) | copy-start | bytes 6148
  19.2 2.5 %copy-start.3 = (bf16[4,1024,2,64]{3,2,1,0:T(2,128)(2,1)S(1)}, bf16[4,1024,2,64]{3,2,1,0:T(2,128)(2,1)}, u32[]{:S(2)}) copy-start(bf16[4,1024,2,64]{3,2,1,0:T(2,128)(2,1)} %get-tuple-element.5) | copy-start | bytes 3145732
  22.7 0.7 copy-start.16
  23.5 3.0 %copy-start.10 = (f32[2048]{0:T(1024)S(1)}, f32[2048]{0:T(1024)}, u32[]{:S(2)}) copy-start(f32[2048]{0:T(1024)} %param.32) | copy-start | bytes 24580
  23.5 3.7 %copy-start.14 = (s32[4,2]{0,1:T(2,128)S(1)}, s32[4,2]{0,1:T(2,128)}, u32[]{:S(2)}) copy-start(s32[4,2]{0,1:T(2,128)} %param.33) | copy-start | bytes 100
  29.3 31.0 %all-to-all-start = ((bf16[128,2,2048]{2,1,0:T(2,128)(2,1)}), bf16[128,2,2048]{2,1,0:T(2,128)(2,1)}, u32[]{:S(2)}, u32[]{:S(2)}) async-start(bf16[128,2,2048]{2,1,0:T(2,128)(2,1)} %bitcast.7), calls=%async_computation | async-start | bytes 2097152 | tf_op jit(solution)/shard_map/all_to_all | solution.py:206
  79.8 34.3 %all-to-all-start.2 = ((bf16[128,2,1024]{2,1,0:T(2,128)(2,1)}), bf16[128,2,1024]{2,1,0:T(2,128)(2,1)}, u32[]{:S(2)}, u32[]{:S(2)}) async-start(bf16[128,2,1024]{2,1,0:T(2,128)(2,1)} %reshape.192), calls=%async_computation.2 | async-start | bytes 1048576 | tf_op jit(solution)/shard_map/all_to_all | solution.py:43
  85.2 24.9 %copy-start.7 = (bf16[1,256,352]{1,2,0:T(8,128)(2,1)S(1)}, bf16[1,256,352]{1,2,0:T(8,128)(2,1)}, u32[]{:S(2)}) copy-start(bf16[1,256,352]{1,2,0:T(8,128)(2,1)} %param.39) | copy-start | bytes 540676
  85.2 25.2 %copy-start.8 = (bf16[1,256,352]{1,2,0:T(8,128)(2,1)S(1)}, bf16[1,256,352]{1,2,0:T(8,128)(2,1)}, u32[]{:S(2)}) copy-start(bf16[1,256,352]{1,2,0:T(8,128)(2,1)} %param.38) | copy-start | bytes 540676
  110.7 9.5 %copy-start.1 = (bf16[128,1,1,2048]{3,2,1,0:T(2,128)(2,1)S(1)}, bf16[128,1,1,2048]{3,2,1,0:T(2,128)(2,1)}, u32[]{:S(2)}) copy-start(bf16[128,1,1,2048]{3,2,1,0:T(2,128)(2,1)} %get-tuple-element.7) | copy-start | bytes 1572868
  114.1 22.2 %all-to-all-start.3 = ((bf16[128,8,352]{2,1,0:T(8,128)(2,1)}), bf16[128,8,352]{2,1,0:T(8,128)(2,1)}, u32[]{:S(2)}, u32[]{:S(2)}) async-start(bf16[128,8,352]{2,1,0:T(8,128)(2,1)} %copy.84), calls=%async_computation.3 | async-start | bytes 1572864 | tf_op jit(solution)/shard_map/all_to_all | solution.py:17
  136.3 18.1 %all-to-all-start.1 = ((bf16[128,2,1024]{2,1,0:T(2,128)(2,1)}), bf16[128,2,1024]{2,1,0:T(2,128)(2,1)S(1)}, u32[]{:S(2)}, u32[]{:S(2)}) async-start(bf16[128,2,1024]{2,1,0:T(2,128)(2,1)} %reshape.194), calls=%async_computation.1 | async-start | bytes 1048576 | tf_op jit(solution)/shard_map/all_to_all | solution.py:43
  142.6 17.2 %copy-start.13 = (bf16[2048]{0:T(1024)(128)(2,1)S(1)}, bf16[2048]{0:T(1024)(128)(2,1)}, u32[]{:S(2)}) copy-start(bf16[2048]{0:T(1024)(128)(2,1)} %param.41) | copy-start | bytes 12292
  142.6 17.2 %copy-start.15 = (f32[4,2]{0,1:T(2,128)S(1)}, f32[4,2]{0,1:T(2,128)}, u32[]{:S(2)}) copy-start(f32[4,2]{0,1:T(2,128)} %param.34) | copy-start | bytes 100
  154.4 5.5 %copy-start.2 = (bf16[128,2,1024]{2,1,0:T(2,128)(2,1)}, bf16[128,2,1024]{2,1,0:T(2,128)(2,1)S(1)}, u32[]{:S(2)}) copy-start(bf16[128,2,1024]{2,1,0:T(2,128)(2,1)S(1)} %all-to-all-done.1) | copy-start | bytes 1572868
  154.4 17.4 %all-to-all-start.4 = ((bf16[128,4,352]{2,1,0:T(4,128)(2,1)}), bf16[128,4,352]{2,1,0:T(4,128)(2,1)}, u32[]{:S(2)}, u32[]{:S(2)}) async-start(bf16[128,4,352]{2,1,0:T(4,128)(2,1)} %copy.87), calls=%async_computation.4 | async-start | bytes 786432 | tf_op jit(solution)/shard_map/all_to_all | solution.py:183
  174.1 17.1 %all-to-all-start.5 = ((bf16[128,4,256]{2,1,0:T(4,128)(2,1)}), bf16[128,4,256]{2,1,0:T(4,128)(2,1)S(1)}, u32[]{:S(2)}, u32[]{:S(2)}) async-start(bf16[128,4,256]{2,1,0:T(4,128)(2,1)} %copy.89), calls=%async_computation.5 | async-start | bytes 524288 | tf_op jit(solution)/shard_map/all_to_all | solution.py:187
Sparse Core Ops, SparseCore 0:
  27.3 77.6 all-gather.2
where the time goes:
time: 200 us; the launch traced here: 199 us
  waiting for transfers between devices  69.5 us (35%)
  starting transfers between devices  39.4 us (20%)
  local copies, waits for them, and re-layouts  37.7 us (19%)
  matrix products  21 us (10%)
  other arithmetic  17 us (8%)
  between operations  14.5 us (7%)
    all_gather x1, waiting for transfers between devices, per_device(): all_rows = lax.all_gather(ffn_in, 'ep', axis=0, tiled=True)  19.9 us
    all_to_all x1, waiting for transfers between devices, per_device(): lax.all_to_all(outgoing, 'ep', split_axis=0, concat_axis=0, tiled=True)  19 us
    unnamed x46, local copies, waits for them, and re-layouts  15.6 us
    all_to_all x1, starting transfers between devices, per_device(): lax.all_to_all(outgoing, 'ep', split_axis=0, concat_axis=0, tiled=True)  12 us
    all_to_all x2, waiting for transfers between devices, exchange_in_pieces(): lax.all_to_all(piece, axis, split_axis=0, concat_axis=0, tiled=True)  10.5 us
    all_to_all x2, starting transfers between devices, exchange_in_pieces(): lax.all_to_all(piece, axis, split_axis=0, concat_axis=0, tiled=True)  9.93 us
    all_to_all x1, waiting for transfers between devices, sent_together(): lax.all_to_all(both, axis, split_axis=split_dim, concat_axis=concat_dim,...  9.43 us
    split x2, other arithmetic, exchange_in_pieces(): jnp.split(tiles, cut_rows(tiles.shape[cut], pieces), axis=cut)  9.13 us
  transfers between devices with their start and end apart: 7, of which 6 were waited for; matrix products, arithmetic and copies ran while one was open for 26% of the time, Pallas kernels for 0%

commit v1 on v0

--- a/solution.py
+++ b/solution.py
@@ -155,7 +155,9 @@
     row_blocks = devices // SPLIT
     capacity = min(SEQ_DEV, max(2, SEQ_DEV * TOP_K * 2 // experts))
     slots = jnp.arange(capacity, dtype=jnp.int32)
-    all_rows = lax.all_gather(ffn_in, "ep", axis=0, tiled=True)
+    all_rows = jnp.concatenate(
+        lax.all_to_all(jnp.stack([ffn_in] * lax.axis_size("ep")), "ep", 0, 0), axis=0
+    )
     gate = jax.nn.sigmoid(jnp.dot(ffn_in, branch_gate, preferred_element_type=jnp.float32))
     position = lax.axis_index("ep")
     row_span = dense_gate.shape[1]

time: 200 us -> 188 us (0.940)
  blocking collectives: 0 us -> 30.6 us
  waiting for transfers between devices: 69.5 us -> 45.7 us
  between operations: 14.5 us -> 1.2 us
  starting transfers between devices: 39.4 us -> 32.8 us
    all_to_all x0 -> x1, blocking collectives: none -> 30.6 us  [per_device(): lax.all_to_all(outgoing, 'ep', split_axis=0, concat_axis=0, tiled=True)]
    all_gather x1 -> x0, waiting for transfers between devices: 19.9 us -> none  [per_device(): all_rows = lax.all_gather(ffn_in, 'ep', axis=0, tiled=True)]
    all_to_all x1, waiting for transfers between devices: 19 us -> 11.8 us  [per_device(): lax.all_to_all(jnp.stack([ffn_in] * lax.axis_size('ep')), 'ep', 0, 0)]
    all_to_all x1, starting transfers between devices: 12 us -> 5.49 us  [per_device(): lax.all_to_all(jnp.stack([ffn_in] * lax.axis_size('ep')), 'ep', 0, 0)]
    all_to_all x2, waiting for transfers between devices: 10.5 us -> 14.8 us  [exchange_in_pieces(): lax.all_to_all(piece, axis, split_axis=0, concat_axis=0, tiled=True)]
    reshape x0 -> x1, local copies, waits for them, and re-layouts: none -> 3.99 us  [per_device(): jnp.concatenate(lax.all_to_all(jnp.stack([ffn_in] * lax.axis_size('ep')),...]
    unnamed x46 -> x63, local copies, waits for them, and re-layouts: 15.6 us -> 11.9 us
    another operation x0 -> x1, local copies, waits for them, and re-layouts: none -> 2.36 us  [per_device(): jnp.stack([ffn_in] * lax.axis_size('ep'))]
  transfers between devices with their start and end apart: 7 -> 6, of which waited for: 6 -> 6; matrix products, arithmetic and copies ran while one was open for 26% -> 27% of each run, Pallas kernels for 0% -> 0%
where the time goes in v1:
time: 188 us; the launch traced here: 187 us
  waiting for transfers between devices  45.7 us (24%)
  local copies, waits for them, and re-layouts  39.2 us (21%)
  starting transfers between devices  32.8 us (17%)
  blocking collectives  30.6 us (16%)
  matrix products  20.4 us (11%)
  other arithmetic  17.1 us (9%)
    all_to_all x1, blocking collectives, per_device(): lax.all_to_all(outgoing, 'ep', split_axis=0, concat_axis=0, tiled=True)  30.6 us
    all_to_all x2, waiting for transfers between devices, exchange_in_pieces(): lax.all_to_all(piece, axis, split_axis=0, concat_axis=0, tiled=True)  14.8 us
    unnamed x63, local copies, waits for them, and re-layouts  11.9 us
    all_to_all x1, waiting for transfers between devices, per_device(): lax.all_to_all(jnp.stack([ffn_in] * lax.axis_size('ep')), 'ep', 0, 0)  11.8 us
    all_to_all x2, starting transfers between devices, exchange_in_pieces(): lax.all_to_all(piece, axis, split_axis=0, concat_axis=0, tiled=True)  9.93 us
    all_to_all x1, waiting for transfers between devices, sent_together(): lax.all_to_all(both, axis, split_axis=split_dim, concat_axis=concat_dim,...  9.39 us
    split x2, other arithmetic, exchange_in_pieces(): jnp.split(tiles, cut_rows(tiles.shape[cut], pieces), axis=cut)  9.27 us
    all_to_all x1, starting transfers between devices, per_device(): lax.all_to_all(down_tile.reshape(devices, rows, row_span).astype(jnp.bflo...  6.81 us
  transfers between devices with their start and end apart: 6, of which 6 were waited for; matrix products, arithmetic and copies ran while one was open for 27% of the time, Pallas kernels for 0%

profile of v1, /device:TPU:1, one launch (start us, length us, event | category | flops | bytes accessed | tf_op | source)
XLA Modules:
  0.0 187.0 jit_solution(664203328900374658)
XLA Ops:
  0.6 1.0 fusion.47
  1.7 2.9 %convolution_convert_fusion.5 = bf16[4,1024]{1,0:T(4,128)(2,1)S(1)} fusion(bf16[2048,1024]{1,0:T(8,128)(2,1)} %param.25, bf16[4,2048]{1,0:T(4,128)(2,1)} %param.21, f32[2048]{0:T(1024)} %param.31, f32[4]{0:T(128)S(1)} %add_rsqrt_fusion.2), kind=kOutput, calls=%fused_computation.22 | convolution fusion | flops 16814080 | bytes 4227088 | tf_op jit(solution)/shard_map/dot_general | solution.py:98
  4.6 0.1 iota_compare_fusion
  4.7 6.7 %fusion.79 = (bf16[4,1024,2,64]{3,2,1,0:T(2,128)(2,1)}, bf16[4,1024,2,64]{3,2,1,0:T(2,128)(2,1)}) fusion(bf16[4,1024,2,128]{3,2,1,0:T(2,128)(2,1)} %param.23), kind=kLoop, calls=%fused_computation.114 | loop fusion | bytes 4194304 | tf_op jit(solution)/shard_map/slice | solution.py:127
  11.5 0.3 convolution_convert_fusion.7
  11.8 0.1 slice_bitcast_fusion
  11.8 0.1 fusion.54
  12.0 0.4 copy-done.15
  12.3 0.2 fusion.51
  12.5 0.1 mul.148
  12.6 0.3 convolution_convert_fusion.6
  12.9 2.5 %select_reduce_fusion.1 = (f32[4,2,4]{2,1,0:T(2,128)S(1)}, f32[4,2,4,1024]{3,2,1,0:T(4,128)S(1)}) fusion(pred[4,1024]{1,0:T(4,128)(4,1)S(1)} %iota_compare_fusion, bf16[4,1024,2,64]{3,2,1,0:T(2,128)(2,1)} %get-tuple-element.6, bf16[4,2,4,128]{3,2,1,0:T(4,128)(2,1)S(1)} %reshape.164), kind=kOutput, calls=%fused_computation.52 | convolution fusion | flops 4292576 | bytes 1192064 | tf_op jit(solution)/shard_map/sgqd,spgd->sgqp/dot_general | solution.py:106
  15.4 0.8 fusion.37
  16.2 0.2 fusion.38
  16.5 0.6 multiply_reduce_fusion.1
  17.1 0.1 multiply_convert_fusion.2
  17.2 3.0 %multiply_reduce_fusion = (f32[4]{0:T(128)S(1)}, f32[4,2048]{1,0:T(4,128)S(1)}) fusion(bf16[4,1024]{1,0:T(4,128)(2,1)S(1)} %reshape.166, bf16[1024,2048]{1,0:T(8,128)(2,1)} %param.28, bf16[4,2048]{1,0:T(4,128)(2,1)S(1)} %copy-done.6), kind=kOutput, calls=%fused_computation.70 | convolution fusion | flops 16809980 | bytes 4251664 | tf_op jit(solution)/shard_map/dot_general | solution.py:151
  20.2 0.1 fusion.58
  20.4 0.1 multiply_convert_fusion.1
  20.5 0.2 convolution_convert_fusion.1
  20.8 0.6 broadcast_in_dim.69
  21.4 30.6 %all_to_all.35 = bf16[128,2,2048]{2,1,0:T(2,128)(2,1)} all-to-all(bf16[128,2,2048]{2,1,0:T(2,128)(2,1)S(1)} %bitcast.73), channel_id=1, replica_groups=mesh['ep'=128] {'ep'}, dimensions={0} | all-to-all | bytes 2097152 | tf_op jit(solution)/shard_map/all_to_all | solution.py:208
  52.0 2.4 %stack.2 = bf16[128,4,2048]{2,1,0:T(4,128)(2,1)} broadcast(bf16[4,2048]{1,0:T(4,128)(2,1)S(1)} %multiply_convert_fusion.1), dimensions={1,2} | broadcast | bytes 2113536 | tf_op jit(solution)/shard_map/stack | solution.py:159
  54.4 5.5 %all-to-all-start.3 = ((bf16[128,4,2048]{2,1,0:T(4,128)(2,1)}), bf16[128,4,2048]{2,1,0:T(4,128)(2,1)}, u32[]{:S(2)}, u32[]{:S(2)}) async-start(bf16[128,4,2048]{2,1,0:T(4,128)(2,1)} %stack.2), calls=%async_computation.3 | async-start | bytes 4194304 | tf_op jit(solution)/shard_map/all_to_all | solution.py:159
  59.9 1.5 reshape.168
  61.4 2.1 %fusion.82 = f32[256,384]{1,0:T(8,128)S(1)} fusion(bf16[256,2048]{1,0:T(8,128)(2,1)S(1)} %reshape.168, bf16[2048,384]{1,0:T(8,128)(2,1)} %param.35), kind=kOutput, calls=%fused_computation.117 | convolution fusion | flops 402653184 | bytes 3014656 | tf_op jit(solution)/shard_map/dot_general | solution.py:62
  63.5 4.2 %convolution_convert_fusion = bf16[256,2048]{1,0:T(8,128)(2,1)} fusion(bf16[384,2048]{1,0:T(8,128)(2,1)} %param.37, bf16[256,2048]{1,0:T(8,128)(2,1)S(1)} %reshape.168, bf16[2048,384]{1,0:T(8,128)(2,1)} %param.36, f32[256,384]{1,0:T(8,128)S(1)} %fusion.82), kind=kOutput, calls=%fused_computation | convolution fusion | flops 806420480 | bytes 5636096 | tf_op jit(solution)/shard_map/dot_general | solution.py:65
  67.7 1.7 convert_element_type.121
  69.4 2.5 %fusion.80 = (bf16[128,1,1,2048]{3,2,1,0:T(2,128)(2,1)}, bf16[128,1,1,2048]{3,2,1,0:T(2,128)(2,1)}) fusion(bf16[128,1,2,2048]{3,2,1,0:T(2,128)(2,1)S(1)} %bitcast.71), kind=kLoop, calls=%fused_computation.115 | loop fusion | bytes 2097152 | tf_op jit(solution)/shard_map/split | solution.py:41
  71.9 0.5 broadcast.144
  72.4 4.8 %reduce = bf16[128,2048]{1,0:T(8,128)(2,1)S(1)} reduce(bf16[128,1,1,2048]{3,2,1,0:T(2,128)(2,1)} %get-tuple-element.8, bf16[]{:T(256)} %broadcast.144), dimensions={1,2}, to_apply=%get-tuple-element.8.reduce_sub_computation | reduce | bytes 1048578 | tf_op jit(solution)/shard_map/split | solution.py:41
  77.2 1.2 reshape.196
  78.3 11.8 %all-to-all-done.3 = bf16[128,4,2048]{2,1,0:T(4,128)(2,1)} async-done(((bf16[128,4,2048]{2,1,0:T(4,128)(2,1)}), bf16[128,4,2048]{2,1,0:T(4,128)(2,1)}, u32[]{:S(2)}, u32[]{:S(2)}) %all-to-all-start.3) | async-done | bytes 2097184 | tf_op jit(solution)/shard_map/all_to_all | solution.py:159
  90.1 5.4 %all-to-all-start.2 = ((bf16[128,2,1024]{2,1,0:T(2,128)(2,1)}), bf16[128,2,1024]{2,1,0:T(2,128)(2,1)}, u32[]{:S(2)}, u32[]{:S(2)}) async-start(bf16[128,2,1024]{2,1,0:T(2,128)(2,1)} %reshape.196), calls=%async_computation.2 | async-start | bytes 1048576 | tf_op jit(solution)/shard_map/all_to_all | solution.py:43
  95.6 4.0 %reshape.169 = bf16[512,2048]{1,0:T(8,128)(2,1)} reshape(bf16[128,4,2048]{2,1,0:T(4,128)(2,1)} %all-to-all-done.3) | data formatting | bytes 4194304 | tf_op jit(solution)/shard_map/reshape | solution.py:158
  99.6 1.0 constant_dynamic-slice_fusion
  100.6 0.3 convolution_convert_fusion.2
  100.9 0.3 convolution_convert_fusion.3
  101.2 0.9 pad_maximum_fusion.1
  102.2 2.4 %copy.84 = bf16[128,8,352]{2,1,0:T(8,128)(2,1)} copy(bf16[128,8,352]{0,2,1:T(8,128)(2,1)} %pad_maximum_fusion.1) | data formatting | bytes 1441792 | tf_op jit(solution)/shard_map/concatenate | solution.py:16
  104.6 4.3 %all-to-all-done.2 = bf16[128,2,1024]{2,1,0:T(2,128)(2,1)} async-done(((bf16[128,2,1024]{2,1,0:T(2,128)(2,1)}), bf16[128,2,1024]{2,1,0:T(2,128)(2,1)}, u32[]{:S(2)}, u32[]{:S(2)}) %all-to-all-start.2) | async-done | bytes 524320 | tf_op jit(solution)/shard_map/all_to_all | solution.py:43
  108.9 6.0 %all-to-all-start.4 = ((bf16[128,8,352]{2,1,0:T(8,128)(2,1)}), bf16[128,8,352]{2,1,0:T(8,128)(2,1)}, u32[]{:S(2)}, u32[]{:S(2)}) async-start(bf16[128,8,352]{2,1,0:T(8,128)(2,1)} %copy.84), calls=%async_computation.4 | async-start | bytes 1572864 | tf_op jit(solution)/shard_map/all_to_all | solution.py:17
  114.9 4.5 %reduce.1 = bf16[128,2048]{1,0:T(8,128)(2,1)} reduce(bf16[128,1,1,2048]{3,2,1,0:T(2,128)(2,1)S(1)} %copy-done.1, bf16[]{:T(256)} %broadcast.144), dimensions={1,2}, to_apply=%get-tuple-element.7.reduce_sub_computation | reduce | bytes 1048578 | tf_op jit(solution)/shard_map/split | solution.py:41
  119.4 2.2 %reshape.198 = bf16[128,2,1024]{2,1,0:T(2,128)(2,1)} reshape(bf16[128,2048]{1,0:T(8,128)(2,1)} %reduce.1) | data formatting | bytes 1048576
  121.7 9.4 %all-to-all-done.4 = bf16[128,8,352]{2,1,0:T(8,128)(2,1)} async-done(((bf16[128,8,352]{2,1,0:T(8,128)(2,1)}), bf16[128,8,352]{2,1,0:T(8,128)(2,1)}, u32[]{:S(2)}, u32[]{:S(2)}) %all-to-all-start.4) | async-done | bytes 720928 | tf_op jit(solution)/shard_map/all_to_all | solution.py:17
  131.0 4.5 %all-to-all-start.1 = ((bf16[128,2,1024]{2,1,0:T(2,128)(2,1)}), bf16[128,2,1024]{2,1,0:T(2,128)(2,1)S(1)}, u32[]{:S(2)}, u32[]{:S(2)}) async-start(bf16[128,2,1024]{2,1,0:T(2,128)(2,1)} %reshape.198), calls=%async_computation.1 | async-start | bytes 1048576 | tf_op jit(solution)/shard_map/all_to_all | solution.py:43
  135.6 1.7 fusion.81
  137.4 0.1 convert_reduce_fusion.1
  137.6 1.0 copy.87
  138.7 10.5 %all-to-all-done.1 = bf16[128,2,1024]{2,1,0:T(2,128)(2,1)S(1)} async-done(((bf16[128,2,1024]{2,1,0:T(2,128)(2,1)}), bf16[128,2,1024]{2,1,0:T(2,128)(2,1)S(1)}, u32[]{:S(2)}, u32[]{:S(2)}) %all-to-all-start.1) | async-done | bytes 524320 | tf_op jit(solution)/shard_map/all_to_all | solution.py:43
  149.2 4.6 %all-to-all-start.5 = ((bf16[128,4,352]{2,1,0:T(4,128)(2,1)}), bf16[128,4,352]{2,1,0:T(4,128)(2,1)S(1)}, u32[]{:S(2)}, u32[]{:S(2)}) async-start(bf16[128,4,352]{2,1,0:T(4,128)(2,1)} %copy.87), calls=%async_computation.5 | async-start | bytes 786432 | tf_op jit(solution)/shard_map/all_to_all | solution.py:185
  153.8 0.7 select_reduce_fusion.2
  154.5 0.6 fusion.22
  155.1 3.6 %reshape.197 = bf16[128,1,1,2048]{3,2,1,0:T(2,128)(2,1)S(1)} reshape(bf16[128,2,1024]{2,1,0:T(2,128)(2,1)} %all-to-all-done.2) | data formatting | bytes 1048576
  158.7 4.3 %reshape.199 = bf16[128,1,1,2048]{3,2,1,0:T(2,128)(2,1)} reshape(bf16[128,2,1024]{2,1,0:T(2,128)(2,1)} %copy-done.2) | data formatting | bytes 1048576
  163.0 3.0 %all-to-all-done.5 = bf16[128,4,352]{2,1,0:T(4,128)(2,1)S(1)} async-done(((bf16[128,4,352]{2,1,0:T(4,128)(2,1)}), bf16[128,4,352]{2,1,0:T(4,128)(2,1)S(1)}, u32[]{:S(2)}, u32[]{:S(2)}) %all-to-all-start.5) | async-done | bytes 360480 | tf_op jit(solution)/shard_map/all_to_all | solution.py:185
  166.0 1.2 convolution_convert_fusion.4
  167.2 0.9 copy.89
  168.1 6.8 %all-to-all-start.6 = ((bf16[128,4,256]{2,1,0:T(4,128)(2,1)}), bf16[128,4,256]{2,1,0:T(4,128)(2,1)S(1)}, u32[]{:S(2)}, u32[]{:S(2)}) async-start(bf16[128,4,256]{2,1,0:T(4,128)(2,1)} %copy.89), calls=%async_computation.6 | async-start | bytes 524288 | tf_op jit(solution)/shard_map/all_to_all | solution.py:189
  175.0 3.5 %pad_maximum_fusion = bf16[128,1,2,2048]{3,2,1,0:T(2,128)(2,1)S(1)} fusion(bf16[128,1,1,2048]{3,2,1,0:T(2,128)(2,1)S(1)} %reshape.197, bf16[128,1,1,2048]{3,2,1,0:T(2,128)(2,1)} %reshape.199), kind=kLoop, calls=%fused_computation.30 | loop fusion | flops 2097152 | bytes 2097152 | tf_op jit(solution)/shard_map/concatenate | solution.py:44
  178.5 0.8 convert_reduce_fusion
  179.3 6.7 %all-to-all-done.6 = bf16[128,4,256]{2,1,0:T(4,128)(2,1)S(1)} async-done(((bf16[128,4,256]{2,1,0:T(4,128)(2,1)}), bf16[128,4,256]{2,1,0:T(4,128)(2,1)S(1)}, u32[]{:S(2)}, u32[]{:S(2)}) %all-to-all-start.6) | async-done | bytes 262176 | tf_op jit(solution)/shard_map/all_to_all | solution.py:189
  186.0 0.1 convert_reduce_fusion.3
  186.2 0.9 fusion.2
  (75 shorter events, 0.7 us)
Async XLA Ops:
  0.6 15.8 %copy-start = (bf16[4,1024,2,128]{3,2,1,0:T(2,128)(2,1)S(1)}, bf16[4,1024,2,128]{3,2,1,0:T(2,128)(2,1)}, u32[]{:S(2)}) copy-start(bf16[4,1024,2,128]{3,2,1,0:T(2,128)(2,1)} %param.24) | copy-start | bytes 6291460
  1.7 2.9 %copy-start.26 = (s32[4]{0:T(128)S(1)}, s32[4]{0:T(128)}, u32[]{:S(2)}) copy-start(s32[4]{0:T(128)} %param.22) | copy-start | bytes 52
  4.7 6.8 %copy-start.4 = (bf16[2048,256]{1,0:T(8,128)(2,1)S(1)}, bf16[2048,256]{1,0:T(8,128)(2,1)}, u32[]{:S(2)}) copy-start(bf16[2048,256]{1,0:T(8,128)(2,1)} %param.26) | copy-start | bytes 3145732
  4.7 6.8 %copy-start.6 = (bf16[4,2048]{1,0:T(4,128)(2,1)S(1)}, bf16[4,2048]{1,0:T(4,128)(2,1)}, u32[]{:S(2)}) copy-start(bf16[4,2048]{1,0:T(4,128)(2,1)} %param.21) | copy-start | bytes 49156
  4.7 6.8 %copy-start.11 = (f32[2048]{0:T(1024)S(1)}, f32[2048]{0:T(1024)}, u32[]{:S(2)}) copy-start(f32[2048]{0:T(1024)} %param.31) | copy-start | bytes 24580
  4.7 7.8 %copy-start.27 = (f32[8]{0:T(128)S(1)}, f32[8]{0:T(128)}, u32[]{:S(2)}) copy-start(f32[8]{0:T(128)} %param.29) | copy-start | bytes 100
  4.7 7.9 %copy-start.5 = (bf16[2048,256]{1,0:T(8,128)(2,1)S(1)}, bf16[2048,256]{1,0:T(8,128)(2,1)}, u32[]{:S(2)}) copy-start(bf16[2048,256]{1,0:T(8,128)(2,1)} %param.27) | copy-start | bytes 3145732
  11.7 0.6 copy-start.15
  12.9 3.3 %copy-start.14 = (bf16[4,256]{1,0:T(4,128)(2,1)}, bf16[4,256]{1,0:T(4,128)(2,1)S(1)}, u32[]{:S(2)}) copy-start(bf16[4,256]{1,0:T(4,128)(2,1)S(1)} %convolution_convert_fusion.6) | copy-start | bytes 6148
  12.9 2.5 %copy-start.3 = (bf16[4,1024,2,64]{3,2,1,0:T(2,128)(2,1)S(1)}, bf16[4,1024,2,64]{3,2,1,0:T(2,128)(2,1)}, u32[]{:S(2)}) copy-start(bf16[4,1024,2,64]{3,2,1,0:T(2,128)(2,1)} %get-tuple-element.5) | copy-start | bytes 3145732
  16.5 0.7 copy-start.24
  17.2 3.0 %copy-start.21 = (s32[4,2]{0,1:T(2,128)S(1)}, s32[4,2]{0,1:T(2,128)}, u32[]{:S(2)}) copy-start(s32[4,2]{0,1:T(2,128)} %param.33) | copy-start | bytes 100
  17.2 3.2 %copy-start.17 = (f32[2048]{0:T(1024)S(1)}, f32[2048]{0:T(1024)}, u32[]{:S(2)}) copy-start(f32[2048]{0:T(1024)} %param.32) | copy-start | bytes 24580
  20.2 34.2 %copy-start.7 = (f32[4,2048]{1,0:T(4,128)}, f32[4,2048]{1,0:T(4,128)S(1)}, u32[]{:S(2)}) copy-start(f32[4,2048]{1,0:T(4,128)S(1)} %get-tuple-element.24) | copy-start | bytes 98308
  20.3 34.0 %copy-start.18 = (pred[8,4]{0,1:T(4,128)(4,1)}, pred[8,4]{0,1:T(4,128)(4,1)S(1)}, u32[]{:S(2)}) copy-start(pred[8,4]{0,1:T(4,128)(4,1)S(1)} %get-tuple-element.16) | copy-start | bytes 100
  20.4 34.0 %copy-start.12 = (s32[8,4]{0,1:T(4,128)}, s32[8,4]{0,1:T(4,128)S(1)}, u32[]{:S(2)}) copy-start(s32[8,4]{0,1:T(4,128)S(1)} %broadcast_add_fusion) | copy-start | bytes 388
  54.4 35.7 %all-to-all-start.3 = ((bf16[128,4,2048]{2,1,0:T(4,128)(2,1)}), bf16[128,4,2048]{2,1,0:T(4,128)(2,1)}, u32[]{:S(2)}, u32[]{:S(2)}) async-start(bf16[128,4,2048]{2,1,0:T(4,128)(2,1)} %stack.2), calls=%async_computation.3 | async-start | bytes 4194304 | tf_op jit(solution)/shard_map/all_to_all | solution.py:159
  90.1 18.8 %all-to-all-start.2 = ((bf16[128,2,1024]{2,1,0:T(2,128)(2,1)}), bf16[128,2,1024]{2,1,0:T(2,128)(2,1)}, u32[]{:S(2)}, u32[]{:S(2)}) async-start(bf16[128,2,1024]{2,1,0:T(2,128)(2,1)} %reshape.196), calls=%async_computation.2 | async-start | bytes 1048576 | tf_op jit(solution)/shard_map/all_to_all | solution.py:43
  95.5 5.1 %copy-start.9 = (bf16[1,256,352]{1,2,0:T(8,128)(2,1)S(1)}, bf16[1,256,352]{1,2,0:T(8,128)(2,1)}, u32[]{:S(2)}) copy-start(bf16[1,256,352]{1,2,0:T(8,128)(2,1)} %param.39) | copy-start | bytes 540676
  95.5 5.3 %copy-start.10 = (bf16[1,256,352]{1,2,0:T(8,128)(2,1)S(1)}, bf16[1,256,352]{1,2,0:T(8,128)(2,1)}, u32[]{:S(2)}) copy-start(bf16[1,256,352]{1,2,0:T(8,128)(2,1)} %param.38) | copy-start | bytes 540676
  101.2 13.7 %copy-start.1 = (bf16[128,1,1,2048]{3,2,1,0:T(2,128)(2,1)S(1)}, bf16[128,1,1,2048]{3,2,1,0:T(2,128)(2,1)}, u32[]{:S(2)}) copy-start(bf16[128,1,1,2048]{3,2,1,0:T(2,128)(2,1)} %get-tuple-element.7) | copy-start | bytes 1572868
  108.9 22.1 %all-to-all-start.4 = ((bf16[128,8,352]{2,1,0:T(8,128)(2,1)}), bf16[128,8,352]{2,1,0:T(8,128)(2,1)}, u32[]{:S(2)}, u32[]{:S(2)}) async-start(bf16[128,8,352]{2,1,0:T(8,128)(2,1)} %copy.84), calls=%async_computation.4 | async-start | bytes 1572864 | tf_op jit(solution)/shard_map/all_to_all | solution.py:17
  131.0 18.1 %all-to-all-start.1 = ((bf16[128,2,1024]{2,1,0:T(2,128)(2,1)}), bf16[128,2,1024]{2,1,0:T(2,128)(2,1)S(1)}, u32[]{:S(2)}, u32[]{:S(2)}) async-start(bf16[128,2,1024]{2,1,0:T(2,128)(2,1)} %reshape.198), calls=%async_computation.1 | async-start | bytes 1048576 | tf_op jit(solution)/shard_map/all_to_all | solution.py:43
  137.3 16.5 %copy-start.20 = (bf16[2048]{0:T(1024)(128)(2,1)S(1)}, bf16[2048]{0:T(1024)(128)(2,1)}, u32[]{:S(2)}) copy-start(bf16[2048]{0:T(1024)(128)(2,1)} %param.41) | copy-start | bytes 12292
  137.3 16.5 %copy-start.22 = (s32[4,2]{0,1:T(2,128)S(1)}, s32[4,2]{0,1:T(2,128)}, u32[]{:S(2)}) copy-start(s32[4,2]{0,1:T(2,128)} %param.33) | copy-start | bytes 100
  137.3 16.5 %copy-start.23 = (f32[4,2]{0,1:T(2,128)S(1)}, f32[4,2]{0,1:T(2,128)}, u32[]{:S(2)}) copy-start(f32[4,2]{0,1:T(2,128)} %param.34) | copy-start | bytes 100
  149.2 5.3 %copy-start.2 = (bf16[128,2,1024]{2,1,0:T(2,128)(2,1)}, bf16[128,2,1024]{2,1,0:T(2,128)(2,1)S(1)}, u32[]{:S(2)}) copy-start(bf16[128,2,1024]{2,1,0:T(2,128)(2,1)S(1)} %all-to-all-done.1) | copy-start | bytes 1572868
  149.2 16.8 %all-to-all-start.5 = ((bf16[128,4,352]{2,1,0:T(4,128)(2,1)}), bf16[128,4,352]{2,1,0:T(4,128)(2,1)S(1)}, u32[]{:S(2)}, u32[]{:S(2)}) async-start(bf16[128,4,352]{2,1,0:T(4,128)(2,1)} %copy.87), calls=%async_computation.5 | async-start | bytes 786432 | tf_op jit(solution)/shard_map/all_to_all | solution.py:185
  168.1 17.9 %all-to-all-start.6 = ((bf16[128,4,256]{2,1,0:T(4,128)(2,1)}), bf16[128,4,256]{2,1,0:T(4,128)(2,1)S(1)}, u32[]{:S(2)}, u32[]{:S(2)}) async-start(bf16[128,4,256]{2,1,0:T(4,128)(2,1)} %copy.89), calls=%async_computation.6 | async-start | bytes 524288 | tf_op jit(solution)/shard_map/all_to_all | solution.py:189
  174.9 11.2 %copy-start.8 = (f32[4,2048]{1,0:T(4,128)S(1)}, f32[4,2048]{1,0:T(4,128)}, u32[]{:S(2)}) copy-start(f32[4,2048]{1,0:T(4,128)} %copy-done.7) | copy-start | bytes 98308
  174.9 11.2 %copy-start.13 = (s32[8,4]{0,1:T(4,128)S(1)}, s32[8,4]{0,1:T(4,128)}, u32[]{:S(2)}) copy-start(s32[8,4]{0,1:T(4,128)} %copy-done.12) | copy-start | bytes 388
  175.0 11.2 %copy-start.16 = (f32[8,4]{0,1:T(4,128)S(1)}, f32[8,4]{0,1:T(4,128)}, u32[]{:S(2)}) copy-start(f32[8,4]{0,1:T(4,128)} %select_reduce_fusion.2) | copy-start | bytes 388
  175.0 11.2 %copy-start.19 = (pred[8,4]{0,1:T(4,128)(4,1)S(1)}, pred[8,4]{0,1:T(4,128)(4,1)}, u32[]{:S(2)}) copy-start(pred[8,4]{0,1:T(4,128)(4,1)} %copy-done.18) | copy-start | bytes 100
  175.0 11.2 %copy-start.25 = (f32[4]{0:T(128)S(1)}, f32[4]{0:T(128)}, u32[]{:S(2)}) copy-start(f32[4]{0:T(128)} %fusion.22) | copy-start | bytes 52
